TPU v7x, 32 devices: a whole 2x2x4 slice. The times are simulated.
32 devices in a mesh: sp: 4 (over z), fs: 4 (over y, x), tp: 2 (over core).
Axes of the slice: x: 2, y: 2, z: 4, core: 2. Of those that a mesh axis runs over, the one named last changes fastest.
Arguments:
- tokens: bfloat16 [4, 1024, 2048], P('fs', 'sp'), may hold values from -6 to 6
- norm_gain: float32 [2048], replicated, may hold values from 0.1 to 1.9
- query_weight: bfloat16 [2048, 1024], P(('sp', 'fs'), 'tp'), may hold values from -0.125 to 0.125
- key_weight: bfloat16 [2048, 1024], P(('sp', 'fs'), 'tp'), may hold values from -0.125 to 0.125
- value_weight: bfloat16 [2048, 1024], P(('sp', 'fs'), 'tp'), may hold values from -0.125 to 0.125
- outgate_weight: bfloat16 [2048, 1024], P(('sp', 'fs'), 'tp'), may hold values from -0.125 to 0.125
- gate_weight: bfloat16 [4, 8, 2048], P(None, 'tp'), may hold values from -0.125 to 0.125
- gate_bias: float32 [4, 8], P(None, 'tp'), may hold values from -1 to 100
- decay_extra: float32 [4, 2, 8, 1024], P('fs', None, 'tp', 'sp'), may hold values from -0.75 to 0
- init_memory: float32 [4, 2, 8, 128, 128], P('fs', None, 'tp'), may hold values from -48 to 48
- init_normalizer: float32 [4, 2, 8, 128], P('fs', None, 'tp'), may hold values from -48 to 48
- head_gain: float32 [8, 128], P('tp'), may hold values from 0.1 to 1.9
- pool_weight: bfloat16 [2048, 2048], P(('sp', 'fs'), 'tp'), may hold values from -0.125 to 0.125
- mem_out_weight: bfloat16 [2048, 1024], P(('sp', 'fs'), 'tp'), may hold values from -0.1875 to 0.1875
- pool_out_weight: bfloat16 [2048, 2048], P(('sp', 'fs'), 'tp'), may hold values from -0.125 to 0.125
Outputs:
- mixed: bfloat16 [4, 1024, 2048], P('fs', ('sp', 'tp'))
All inputs are finite; a program needn't handle non-finite values.
Results may differ from a plain program's by a relative error of at most 0.014.
Values may be sent and summed in bfloat16 or wider, within the bound.
A program may use at most 64 MiB of HBM per device.

v0:
```python
import math
import jax
import jax.numpy as jnp
from jax import lax
from jax.sharding import PartitionSpec as P

HALO = 8
norm_eps = 1e-06
exact_mode = lax.Precision.HIGHEST


def carried_in(x, axis, combine, identity, reverse):
    length, position = (lax.axis_size(axis), lax.axis_index(axis))
    everything = jax.tree.map(lambda part: lax.all_gather(part, axis), x)
    start = jax.tree.map(
        lambda part, zero: jnp.broadcast_to(jnp.asarray(zero, part.dtype), part.shape), x, identity
    )

    def lap(k, before):
        at = length - 1 - k if reverse else k
        reached = at > position if reverse else at < position
        new = combine(before, jax.tree.map(lambda part: part[at], everything))
        return jax.tree.map(lambda a, b: jnp.where(reached, a, b), new, before)

    return lax.fori_loop(0, length, lap, start)


def padded_2(block, sides, width):
    for axis, dim in sides:
        count = lax.axis_size(axis)
        forward = [(i, i + 1) for i in range(count - 1)]
        backward = [(target, source) for source, target in forward]
        low = lax.ppermute(
            lax.slice_in_dim(block, block.shape[dim] - width, None, axis=dim), axis, forward
        )
        high = lax.ppermute(lax.slice_in_dim(block, 0, width, axis=dim), axis, backward)
        block = jnp.concatenate([low, block, high], axis=dim)
    return block


def block_output(
    query_rows, key_rows, value_rows, input_gate, log_forget, memory, normalizer, stabilizer
):
    block_len = query_rows.shape[1]
    key_scale = key_rows.shape[-1] ** (-0.5)
    lower_mask = jnp.tril(jnp.ones((block_len, block_len), dtype=bool))
    summed = jnp.cumsum(log_forget, axis=-1)
    log_decay = jnp.where(
        lower_mask, summed[:, :, None] - summed[:, None, :] + input_gate[:, None, :], -jnp.inf
    )
    log_carry = stabilizer[:, None] + summed
    running_max = jnp.maximum(log_carry, jnp.max(log_decay, axis=-1))
    scores = (
        jnp.einsum("btd,bsd->bts", query_rows, key_rows, preferred_element_type=jnp.float32)
        * key_scale
    )
    inner_weight = jnp.exp(log_decay - running_max[:, :, None]) * scores
    weight_rounded = inner_weight.astype(jnp.bfloat16)
    carry_weight = jnp.exp(log_carry - running_max)
    query_wide = query_rows.astype(jnp.float32)
    numerator = carry_weight[:, :, None] * jnp.einsum(
        "bed,btd->bte", memory, query_wide, precision=exact_mode
    )
    numerator = numerator + jnp.einsum(
        "bts,bse->bte", weight_rounded, value_rows, preferred_element_type=jnp.float32
    )
    denominator = carry_weight * jnp.einsum(
        "bd,btd->bt", normalizer, query_wide, precision=exact_mode
    )
    denominator = denominator + jnp.sum(inner_weight, axis=-1)
    return numerator / jnp.maximum(jnp.abs(denominator), jnp.exp(-running_max))[:, :, None]


def block_summary(key_rows, value_rows, input_gate, log_forget):
    key_wide = key_rows.astype(jnp.float32) * key_rows.shape[-1] ** (-0.5)
    summed = jnp.cumsum(log_forget, axis=-1)
    forget_total = summed[:, -1]
    log_weight = forget_total[:, None] - summed + input_gate
    running_max = jnp.max(log_weight, axis=-1)
    weights = jnp.exp(log_weight - running_max[:, None])
    memory = jnp.einsum(
        "bse,bsd->bed",
        weights[:, :, None] * value_rows.astype(jnp.float32),
        key_wide,
        precision=exact_mode,
    )
    normalizer = jnp.einsum("bs,bsd->bd", weights, key_wide, precision=exact_mode)
    return (memory, normalizer, running_max, forget_total)


def combine(earlier, latter):
    early_memory, early_norm, early_max, early_total = earlier
    late_memory, late_norm, late_max, late_total = latter
    joint_max = jnp.maximum(early_max + late_total, late_max)
    early_scale = jnp.exp(early_max + late_total - joint_max)
    late_scale = jnp.exp(late_max - joint_max)
    memory = early_scale[:, None, None] * early_memory + late_scale[:, None, None] * late_memory
    normalizer = early_scale[:, None] * early_norm + late_scale[:, None] * late_norm
    return (memory, normalizer, joint_max, early_total + late_total)


def span_sweep(
    query_rows, key_rows, value_rows, input_gate, log_forget, memory, normalizer, stabilizer, span
):
    block_count = query_rows.shape[1] // span

    def to_blocks(array):
        shaped = array.reshape((array.shape[0], block_count, span) + array.shape[2:])
        return jnp.moveaxis(shaped, 1, 0)

    def advance(carried, pieces):
        query_blk, key_blk, value_blk, gate_blk, forget_blk = pieces
        result = block_output(
            query_blk, key_blk, value_blk, gate_blk, forget_blk, carried[0], carried[1], carried[2]
        )
        return (combine(carried, block_summary(key_blk, value_blk, gate_blk, forget_blk)), result)

    initial = (memory, normalizer, stabilizer, jnp.zeros_like(stabilizer))
    ignored, outputs = lax.scan(
        advance,
        initial,
        tuple(
            (
                to_blocks(array)
                for array in (query_rows, key_rows, value_rows, input_gate, log_forget)
            )
        ),
    )
    return jnp.moveaxis(outputs, 0, 1).reshape(query_rows.shape[:2] + (value_rows.shape[2],))


def reverse_time(array):
    return jnp.flip(array, axis=1)


def to_heads(matrix, head_count):
    shaped = matrix.reshape(matrix.shape[0], head_count, matrix.shape[1] // head_count)
    return shaped.transpose(1, 0, 2)


def pool_window(padded, positions, channels, seq_len, group_size):
    row_count = positions.shape[0]
    group_index = channels // group_size
    reach_left = jnp.left_shift(jnp.ones_like(group_index), group_index)
    reach_right = reach_left - 1
    window_sum = jnp.zeros((row_count, channels.shape[0]), jnp.float32)
    for offset in range(-HALO, HALO):
        inside = ((offset >= -reach_left) & (offset <= reach_right)).astype(jnp.float32)
        window_sum = window_sum + inside * padded[HALO + offset : HALO + offset + row_count]
    first_pos = jnp.maximum(positions[:, None] - reach_left[None, :], 0)
    last_pos = jnp.minimum(positions[:, None] + reach_right[None, :], seq_len - 1)
    counted = (last_pos - first_pos + 1).astype(jnp.float32)
    centre = padded[HALO : HALO + row_count]
    return (window_sum / counted - centre).astype(jnp.bfloat16)


def per_device(
    tokens,
    norm_gain,
    query_weight,
    key_weight,
    value_weight,
    outgate_weight,
    gate_weight,
    gate_bias,
    decay_extra,
    init_memory,
    init_normalizer,
    head_gain,
    pool_weight,
    mem_out_weight,
    pool_out_weight,
):
    block_len = tokens.shape[1]
    model_width = tokens.shape[2]
    head_count, head_width = head_gain.shape
    span = math.gcd(block_len, 256)
    flattened = tokens[0].astype(jnp.float32)
    normed = (
        flattened
        * lax.rsqrt(jnp.mean(flattened * flattened, axis=-1, keepdims=True) + norm_eps)
        * norm_gain
    ).astype(jnp.bfloat16)
    zero_start = tuple(
        (
            jnp.zeros((block_len, weight.shape[1]), jnp.float32)
            for weight in (query_weight, key_weight, value_weight, outgate_weight, pool_weight)
        )
    )
    zero_start = zero_start + (
        jnp.zeros((model_width, mem_out_weight.shape[1]), jnp.bfloat16),
        jnp.zeros((model_width, pool_out_weight.shape[1]), jnp.bfloat16),
    )
    line_query, line_key, line_value, line_outgate, line_pool, line_mem_out, line_pool_out = (
        lax.all_gather(query_weight, "fs", axis=0, tiled=True),
        lax.all_gather(key_weight, "fs", axis=0, tiled=True),
        lax.all_gather(value_weight, "fs", axis=0, tiled=True),
        lax.all_gather(outgate_weight, "fs", axis=0, tiled=True),
        lax.all_gather(pool_weight, "fs", axis=0, tiled=True),
        lax.all_gather(mem_out_weight, "fs", axis=0, tiled=True),
        lax.all_gather(pool_out_weight, "fs", axis=0, tiled=True),
    )
    pieces = (
        lax.all_gather(line_query, "sp", axis=0, tiled=True),
        lax.all_gather(line_key, "sp", axis=0, tiled=True),
        lax.all_gather(line_value, "sp", axis=0, tiled=True),
        lax.all_gather(line_outgate, "sp", axis=0, tiled=True),
        lax.all_gather(line_pool, "sp", axis=0, tiled=True),
        lax.all_gather(line_mem_out, "sp", axis=0, tiled=True),
        lax.all_gather(line_pool_out, "sp", axis=0, tiled=True),
    )
    partial_sums = tuple(
        (
            jnp.dot(normed, weight_rows, preferred_element_type=jnp.float32)
            for weight_rows in pieces[:5]
        )
    )
    collected = tuple((weight_rows for weight_rows in pieces[5:]))
    folded = partial_sums + collected
    query_proj, key_proj, value_proj, outgate, pool_input = tuple(
        (running.astype(jnp.bfloat16) for running in folded[:5])
    )
    mem_weight_all = folded[5]
    pool_weight_all = folded[6]
    gate_pre = lax.dot_general(
        normed,
        gate_weight.reshape(4 * head_count, model_width),
        (((1,), (1,)), ((), ())),
        preferred_element_type=jnp.float32,
    ) + gate_bias.reshape(4 * head_count)
    gate_pre = gate_pre.reshape(block_len, 4, head_count).transpose(1, 2, 0)
    query_heads = to_heads(query_proj, head_count)
    key_heads = to_heads(key_proj, head_count)
    value_heads = to_heads(value_proj, head_count)
    forward_forget = jax.nn.log_sigmoid(gate_pre[1]) + decay_extra[0, 0]
    backward_forget = jax.nn.log_sigmoid(gate_pre[3]) + decay_extra[0, 1]
    zero_rows = jnp.zeros((head_count,), jnp.float32)
    identity = (
        jnp.zeros((head_count, head_width, head_width), jnp.float32),
        jnp.zeros((head_count, head_width), jnp.float32),
        jnp.full((head_count,), -1e30, jnp.float32),
        zero_rows,
    )
    front_memory, front_norm, front_max, front_total = block_summary(
        key_heads, value_heads, gate_pre[0], forward_forget
    )
    prefix = carried_in(
        (front_memory, front_norm, front_max, front_total), "sp", combine, identity, False
    )
    incoming = combine((init_memory[0, 0], init_normalizer[0, 0], zero_rows, zero_rows), prefix)
    forward_out = span_sweep(
        query_heads,
        key_heads,
        value_heads,
        gate_pre[0],
        forward_forget,
        incoming[0],
        incoming[1],
        incoming[2],
        span,
    )
    back_query = reverse_time(query_heads)
    back_key = reverse_time(key_heads)
    back_value = reverse_time(value_heads)
    back_gate = reverse_time(gate_pre[2])
    back_forget = reverse_time(backward_forget)
    rear_memory, rear_norm, rear_max, rear_total = block_summary(
        back_key, back_value, back_gate, back_forget
    )
    suffix = carried_in(
        (rear_memory, rear_norm, rear_max, rear_total), "sp", combine, identity, True
    )
    back_incoming = combine(
        (init_memory[0, 1], init_normalizer[0, 1], zero_rows, zero_rows), suffix
    )
    backward_out = reverse_time(
        span_sweep(
            back_query,
            back_key,
            back_value,
            back_gate,
            back_forget,
            back_incoming[0],
            back_incoming[1],
            back_incoming[2],
            span,
        )
    )
    summed_dirs = (forward_out + backward_out).transpose(1, 0, 2)
    normed_heads = (
        summed_dirs
        * lax.rsqrt(jnp.mean(summed_dirs * summed_dirs, axis=-1, keepdims=True) + norm_eps)
        * head_gain
    )
    out_gate = jax.nn.sigmoid(
        outgate.astype(jnp.float32).reshape(block_len, head_count, head_width)
    )
    memory_out = (
        (normed_heads * out_gate).astype(jnp.bfloat16).reshape(block_len, head_count * head_width)
    )
    padded = padded_2(pool_input, (("sp", 0),), HALO).astype(jnp.float32)
    feature_count = pool_input.shape[1]
    positions = lax.axis_index("sp") * block_len + jnp.arange(block_len, dtype=jnp.int32)
    channels = lax.axis_index("tp") * feature_count + jnp.arange(feature_count, dtype=jnp.int32)
    pool_out = pool_window(
        padded, positions, channels, block_len * lax.axis_size("sp"), model_width // 4
    )
    own_rows = block_len // lax.axis_size("tp")
    result = lax.dot_general(
        memory_out, mem_weight_all, (((1,), (1,)), ((), ())), preferred_element_type=jnp.float32
    )
    mixed = lax.psum_scatter(
        (
            result
            + lax.dot_general(
                pool_out,
                pool_weight_all,
                (((1,), (1,)), ((), ())),
                preferred_element_type=jnp.float32,
            )
        ).astype(jnp.bfloat16),
        "tp",
        scatter_dimension=0,
        tiled=True,
    )
    return mixed.reshape(1, own_rows, model_width)


def solution(mesh):
    placed = (
        P("fs", "sp", None),
        P(),
        P(("sp", "fs"), "tp"),
        P(("sp", "fs"), "tp"),
        P(("sp", "fs"), "tp"),
        P(("sp", "fs"), "tp"),
        P(None, "tp", None),
        P(None, "tp"),
        P("fs", None, "tp", "sp"),
        P("fs", None, "tp", None, None),
        P("fs", None, "tp", None),
        P("tp", None),
        P(("sp", "fs"), "tp"),
        P(("sp", "fs"), "tp"),
        P(("sp", "fs"), "tp"),
    )
    return jax.shard_map(
        per_device,
        mesh=mesh,
        in_specs=placed,
        out_specs=P("fs", ("sp", "tp"), None),
        check_vma=False,
    )
```

profile of v0, /device:TPU:0, one launch (start us, length us, event | category | flops | bytes accessed | tf_op | source)
XLA Modules:
  0.0 544.0 jit_solution(11762868126986876266)
XLA Ops:
  6.5 13.3 %all_gather.89 = bf16[512,512]{1,0:T(8,128)(2,1)} all-gather(bf16[128,512]{1,0:T(8,128)(2,1)} %param.22), channel_id=1, replica_groups=mesh['sp'=4,'fs'=4,'tp'=2] {'fs'}, dimensions={0}, use_global_device_ids=true | all-gather | bytes 655360 | tf_op jit(solution)/shard_map/all_gather | solution.py:196
  19.9 11.6 %all_gather.87 = bf16[512,512]{1,0:T(8,128)(2,1)} all-gather(bf16[128,512]{1,0:T(8,128)(2,1)} %param.23), channel_id=1, replica_groups=mesh['sp'=4,'fs'=4,'tp'=2] {'fs'}, dimensions={0}, use_global_device_ids=true | all-gather | bytes 655360 | tf_op jit(solution)/shard_map/all_gather | solution.py:197
  32.9 10.5 %all_gather.95 = bf16[512,512]{1,0:T(8,128)(2,1)} all-gather(bf16[128,512]{1,0:T(8,128)(2,1)S(1)} %copy-done.3), channel_id=1, replica_groups=mesh['sp'=4,'fs'=4,'tp'=2] {'fs'}, dimensions={0}, use_global_device_ids=true | all-gather | bytes 655360 | tf_op jit(solution)/shard_map/all_gather | solution.py:195
  43.5 10.5 %all_gather.104 = bf16[512,512]{1,0:T(8,128)(2,1)} all-gather(bf16[128,512]{1,0:T(8,128)(2,1)S(1)} %copy-done.4), channel_id=1, replica_groups=mesh['sp'=4,'fs'=4,'tp'=2] {'fs'}, dimensions={0}, use_global_device_ids=true | all-gather | bytes 655360 | tf_op jit(solution)/shard_map/all_gather | solution.py:198
  55.1 1.2 reduce-window.24
  57.2 8.7 %all-gather.24.cloned.1.call-done = bf16[2048,512]{1,0:T(8,128)(2,1)} async-done(((bf16[512,512]{1,0:T(8,128)(2,1)}), bf16[2048,512]{1,0:T(8,128)(2,1)}) %all-gather.24.cloned.1.call-update) | async-done | bytes 2097168 | tf_op jit(solution)/shard_map/all_gather | solution.py:205
  65.9 2.3 fusion.36
  68.3 43.7 %all-gather.22.cloned.1.call-done = bf16[2048,512]{1,0:T(8,128)(2,1)} async-done(((bf16[512,512]{1,0:T(8,128)(2,1)}), bf16[2048,512]{1,0:T(8,128)(2,1)}) %all-gather.22.cloned.1.call-update) | async-done | bytes 2097168 | tf_op jit(solution)/shard_map/all_gather | solution.py:206
  112.0 2.3 fusion.35
  114.3 1.9 fusion.71
  116.5 1.2 reduce-window.26
  119.5 1.9 fusion.65
  121.5 17.7 %all-gather.32.cloned.1.call-done = bf16[512,1024]{1,0:T(8,128)(2,1)} async-done(((bf16[128,1024]{1,0:T(8,128)(2,1)}), bf16[512,1024]{1,0:T(8,128)(2,1)}) %all-gather.32.cloned.1.call-update) | async-done | bytes 1048592 | tf_op jit(solution)/shard_map/all_gather | solution.py:199
  139.3 28.2 %all-gather.36.cloned.1.call-done = bf16[512,1024]{1,0:T(8,128)(2,1)} async-done(((bf16[128,1024]{1,0:T(8,128)(2,1)}), bf16[512,1024]{1,0:T(8,128)(2,1)}) %all-gather.36.cloned.1.call-update) | async-done | bytes 1048592 | tf_op jit(solution)/shard_map/all_gather | solution.py:201
  167.5 10.6 %all_gather.106 = bf16[512,512]{1,0:T(8,128)(2,1)} all-gather(bf16[128,512]{1,0:T(8,128)(2,1)S(1)} %copy-done.5), channel_id=1, replica_groups=mesh['sp'=4,'fs'=4,'tp'=2] {'fs'}, dimensions={0}, use_global_device_ids=true | all-gather | bytes 655360 | tf_op jit(solution)/shard_map/all_gather | solution.py:200
  185.9 12.3 %all-reduce.4 = (f32[16]{0:T(128)S(1)}, f32[16]{0:T(128)S(1)}, f32[16]{0:T(128)S(1)}, f32[16]{0:T(128)S(1)}) all-reduce(f32[16]{0:T(128)S(1)} %dynamic-update-slice.2, f32[16]{0:T(128)S(1)} %dynamic-update-slice.3, f32[16]{0:T(128)S(1)} %dynamic-update-slice, f32[16]{0:T(128)S(1)} %dynamic-update-slice.1), channel_id=6, replica_groups=mesh['sp'=4,'fs'=4,'tp'=2] {'sp'}, use_global_device_ids=true, to_apply=%add.2 | all-reduce | flops 64 | bytes 512
  201.4 12.5 %all-gather.8 = f32[4,4,128]{2,1,0:T(4,128)S(1)} all-gather(f32[1,4,128]{2,1,0:T(4,128)S(1)} %bitcast.306), channel_id=5, replica_groups=mesh['sp'=4,'fs'=4,'tp'=2] {'sp'}, dimensions={0}, use_global_device_ids=true | all-gather | bytes 10240 | tf_op jit(solution)/shard_map/all_gather | solution.py:14
  214.2 12.1 %all-gather.9 = f32[4,4,128]{2,1,0:T(4,128)S(1)} all-gather(f32[1,4,128]{2,1,0:T(4,128)S(1)} %bitcast.302), channel_id=9, replica_groups=mesh['sp'=4,'fs'=4,'tp'=2] {'sp'}, dimensions={0}, use_global_device_ids=true | all-gather | bytes 10240 | tf_op jit(solution)/shard_map/all_gather | solution.py:14
  226.4 2.3 fusion.37
  229.1 31.8 %all-gather.28.cloned.1.call-done = bf16[2048,512]{1,0:T(8,128)(2,1)} async-done(((bf16[512,512]{1,0:T(8,128)(2,1)}), bf16[2048,512]{1,0:T(8,128)(2,1)}) %all-gather.28.cloned.1.call-update) | async-done | bytes 2097168 | tf_op jit(solution)/shard_map/all_gather | solution.py:207
  260.9 3.2 fusion.34
  264.1 1.2 copy.60
  265.4 23.9 %all-gather.40.cloned.1.call-done = f32[16,128,128]{2,1,0:T(8,128)} async-done(((f32[4,128,128]{2,1,0:T(8,128)}), f32[16,128,128]{2,1,0:T(8,128)}) %all-gather.40.cloned.1.call-update) | async-done | bytes 1048592 | tf_op jit(solution)/shard_map/all_gather | solution.py:14
  289.3 7.4 %while.12 = (s32[]{:T(128)}, f32[4,128,128]{2,1,0:T(8,128)S(1)}, f32[4,128]{1,0:T(4,128)S(1)}, f32[4]{0:T(128)S(1)}, f32[4]{0:T(128)S(1)}, /*index=5*/s32[]{:T(1...) while((s32[]{:T(128)}, f32[4,128,128]{2,1,0:T(8,128)S(1)}, ...), condition=%wide.region_5.6_spmd.clone, body=%wide.region_4.5_spmd.clone.sunk | while | flops 330284 | bytes 792973 | solution.py:25
  290.0 1.1 fusion.157
  291.8 1.1 fusion.157
  293.7 1.1 fusion.157
  295.5 1.1 fusion.157
  297.8 2.3 fusion.133
  300.1 18.2 %all-gather.42.cloned.1.call-done = f32[16,128,128]{2,1,0:T(8,128)} async-done(((f32[4,128,128]{2,1,0:T(8,128)}), f32[16,128,128]{2,1,0:T(8,128)}) %all-gather.42.cloned.1.call-update) | async-done | bytes 1048592 | tf_op jit(solution)/shard_map/all_gather | solution.py:14
  318.3 7.5 %while.13 = (s32[]{:T(128)}, f32[4,128,128]{2,1,0:T(8,128)S(1)}, f32[4,128]{1,0:T(4,128)S(1)}, f32[4]{0:T(128)S(1)}, f32[4]{0:T(128)S(1)}, /*index=5*/s32[]{:T(1...) while((s32[]{:T(128)}, f32[4,128,128]{2,1,0:T(8,128)S(1)}, ...), condition=%wide.region_12.13_spmd.clone, body=%wide.region_11.12_spmd.clone.sunk | while | flops 330288 | bytes 793035 | solution.py:25
  319.0 1.1 fusion.159
  320.9 1.1 fusion.159
  322.7 1.1 fusion.159
  324.6 1.1 fusion.159
  327.7 1.2 fusion.25
  329.0 5.0 rev.26
  334.4 1.7 multiply_reduce_fusion
  336.1 63.9 %all-gather.34.cloned.1.call-done = bf16[2048,1024]{1,0:T(8,128)(2,1)} async-done(((bf16[512,1024]{1,0:T(8,128)(2,1)}), bf16[2048,1024]{1,0:T(8,128)(2,1)}) %all-gather.34.cloned.1.call-update) | async-done | bytes 4194320 | tf_op jit(solution)/shard_map/all_gather | solution.py:208
  400.0 3.5 convolution_convert_fusion
  403.7 1.3 collective-permute-start
  405.0 1.3 collective-permute-start.1
  406.4 4.2 collective-permute-done.1
  410.8 69.9 %all-gather.38.cloned.1.call-done = bf16[2048,1024]{1,0:T(8,128)(2,1)} async-done(((bf16[512,1024]{1,0:T(8,128)(2,1)}), bf16[2048,1024]{1,0:T(8,128)(2,1)}) %all-gather.38.cloned.1.call-update) | async-done | bytes 4194320 | tf_op jit(solution)/shard_map/all_gather | solution.py:210
  480.8 5.3 fusion.74
  486.1 40.3 %all-gather.30.cloned.1.call-done = bf16[2048,512]{1,0:T(8,128)(2,1)} async-done(((bf16[512,512]{1,0:T(8,128)(2,1)}), bf16[2048,512]{1,0:T(8,128)(2,1)}) %all-gather.30.cloned.1.call-update) | async-done | bytes 2097168 | tf_op jit(solution)/shard_map/all_gather | solution.py:209
  526.4 3.4 fusion.16
  529.8 7.3 %reduce-scatter.2.cloned.1.call-done = bf16[128,2048]{1,0:T(8,128)(2,1)} async-done(((bf16[256,2048]{1,0:T(8,128)(2,1)}), bf16[128,2048]{1,0:T(8,128)(2,1)}) %reduce-scatter.2.cloned.1.call-update) | async-done | bytes 524304 | tf_op jit(solution)/shard_map/reduce_scatter | solution.py:312
  (220 shorter events, 26.4 us)
Async XLA Ops:
  6.5 26.4 %copy-start.3 = (bf16[128,512]{1,0:T(8,128)(2,1)S(1)}, bf16[128,512]{1,0:T(8,128)(2,1)}, u32[]{:S(2)}) copy-start(bf16[128,512]{1,0:T(8,128)(2,1)} %param.21) | copy-start | bytes 393220
  6.5 37.0 %copy-start.4 = (bf16[128,512]{1,0:T(8,128)(2,1)S(1)}, bf16[128,512]{1,0:T(8,128)(2,1)}, u32[]{:S(2)}) copy-start(bf16[128,512]{1,0:T(8,128)(2,1)} %param.24) | copy-start | bytes 393220
  6.5 59.4 %all-gather.24.cloned.1.call-start = ((), (), s32[]{:S(2)}) async-start(), calls=%async_computation.2 | async-start | bytes 2621440 | tf_op jit(solution)/shard_map/all_gather | solution.py:205
  19.9 34.3 %copy-start.6 = (bf16[4,4,2048]{2,1,0:T(4,128)(2,1)S(1)}, bf16[4,4,2048]{2,1,0:T(4,128)(2,1)}, u32[]{:S(2)}) copy-start(bf16[4,4,2048]{2,1,0:T(4,128)(2,1)} %param.25) | copy-start | bytes 196612
  19.9 34.3 %copy-start.28 = (f32[4,4]{1,0:T(4,128)S(1)}, f32[4,4]{1,0:T(4,128)}, u32[]{:S(2)}) copy-start(f32[4,4]{1,0:T(4,128)} %param.26) | copy-start | bytes 196
  19.9 34.4 %copy-start = (bf16[1,256,2048]{2,1,0:T(8,128)(2,1)S(1)}, bf16[1,256,2048]{2,1,0:T(8,128)(2,1)}, u32[]{:S(2)}) copy-start(bf16[1,256,2048]{2,1,0:T(8,128)(2,1)} %param.19) | copy-start | bytes 3145732
  19.9 92.1 %all-gather.22.cloned.1.call-start = ((), (), s32[]{:S(2)}) async-start(), calls=%async_computation.1 | async-start | bytes 2621440 | tf_op jit(solution)/shard_map/all_gather | solution.py:206
  31.5 23.0 %copy-start.34 = (f32[2048]{0:T(1024)S(1)}, f32[2048]{0:T(1024)}, u32[]{:S(2)}) copy-start(f32[2048]{0:T(1024)} %param.20) | copy-start | bytes 24580
  31.5 107.7 %all-gather.32.cloned.1.call-start = ((), (), s32[]{:S(2)}) async-start(), calls=%async_computation.6 | async-start | bytes 1310720 | tf_op jit(solution)/shard_map/all_gather | solution.py:199
  32.3 135.2 %all-gather.36.cloned.1.call-start = ((), (), s32[]{:S(2)}) async-start(), calls=%async_computation.8 | async-start | bytes 1310720 | tf_op jit(solution)/shard_map/all_gather | solution.py:201
  32.8 193.5 %all-gather.26.cloned.1.call-start = ((), (), s32[]{:S(2)}) async-start(), calls=%async_computation.3 | async-start | bytes 2621440 | tf_op jit(solution)/shard_map/all_gather | solution.py:204
  43.4 11.7 %slice-start = ((f32[1,2,4,256]{3,2,1,0:T(4,128)}), f32[1,1,4,256]{3,2,1,0:T(4,128)S(1)}, s32[]{:S(2)}) async-start(f32[1,2,4,256]{3,2,1,0:T(4,128)} %param.27), calls=%async_computation.13 | async-start | bytes 8192 | tf_op jit(solution)/shard_map/slice | solution.py:235
  43.4 13.7 %copy-start.7 = (f32[1,2,4,256]{3,2,1,0:T(4,128)S(1)}, f32[1,2,4,256]{3,2,1,0:T(4,128)}, u32[]{:S(2)}) copy-start(f32[1,2,4,256]{3,2,1,0:T(4,128)} %param.27) | copy-start | bytes 24580
  43.5 217.5 %all-gather.28.cloned.1.call-start = ((), (), s32[]{:S(2)}) async-start(), calls=%async_computation.4 | async-start | bytes 2621440 | tf_op jit(solution)/shard_map/all_gather | solution.py:207
  54.1 235.2 %all-gather.40.cloned.1.call-start = ((), (), s32[]{:S(2)}) async-start(), calls=%async_computation.11 | async-start | bytes 1310720 | tf_op jit(solution)/shard_map/all_gather | solution.py:14
  54.6 206.3 %copy-start.30 = (f32[256]{0:T(256)}, f32[256]{0:T(256)S(1)}, u32[]{:S(2)}) copy-start(f32[256]{0:T(256)S(1)} %add_rsqrt_fusion.1) | copy-start | bytes 3076
  68.3 132.7 %copy-start.2 = (bf16[32,4,8,128]{3,2,1,0:T(8,128)(2,1)}, bf16[32,4,8,128]{3,2,1,0:T(8,128)(2,1)S(1)}, u32[]{:S(2)}) copy-start(bf16[32,4,8,128]{3,2,1,0:T(8,128)(2,1)S(1)} %fusion.36) | copy-start | bytes 786436
  116.2 202.0 %all-gather.42.cloned.1.call-start = ((), (), s32[]{:S(2)}) async-start(), calls=%async_computation.12 | async-start | bytes 1310720 | tf_op jit(solution)/shard_map/all_gather | solution.py:14
  118.9 48.7 %copy-start.5 = (bf16[128,512]{1,0:T(8,128)(2,1)S(1)}, bf16[128,512]{1,0:T(8,128)(2,1)}, u32[]{:S(2)}) copy-start(bf16[128,512]{1,0:T(8,128)(2,1)} %param.32) | copy-start | bytes 393220
  119.5 64.3 %copy-start.37 = (u32[32]{0:T(128)S(1)}, u32[32]{0:T(128)}, u32[]{:S(2)}) copy-start(u32[32]{0:T(128)} %constant.215) | copy-start | bytes 388
  121.4 278.6 %all-gather.34.cloned.1.call-start = ((), (), s32[]{:S(2)}) async-start(), calls=%async_computation.7 | async-start | bytes 5242880 | tf_op jit(solution)/shard_map/all_gather | solution.py:208
  139.2 341.4 %all-gather.38.cloned.1.call-start = ((), (), s32[]{:S(2)}) async-start(), calls=%async_computation.9 | async-start | bytes 5242880 | tf_op jit(solution)/shard_map/all_gather | solution.py:210
  167.5 358.9 %all-gather.30.cloned.1.call-start = ((), (), s32[]{:S(2)}) async-start(), calls=%async_computation.5 | async-start | bytes 2621440 | tf_op jit(solution)/shard_map/all_gather | solution.py:209
  178.2 359.0 %reduce-scatter.2.cloned.1.call-start = ((), (), s32[]{:S(2)}) async-start(), calls=%async_computation.10 | async-start | bytes 1572864 | tf_op jit(solution)/shard_map/reduce_scatter | solution.py:312
  334.1 65.9 %copy-start.31 = (f32[256]{0:T(256)S(1)}, f32[256]{0:T(256)}, u32[]{:S(2)}) copy-start(f32[256]{0:T(256)} %copy-done.30) | copy-start | bytes 3076
  334.1 65.9 %copy-start.35 = (f32[2048]{0:T(1024)S(1)}, f32[2048]{0:T(1024)}, u32[]{:S(2)}) copy-start(f32[2048]{0:T(1024)} %param.20) | copy-start | bytes 24580
  336.1 70.2 %copy-start.27 = (f32[4,128]{1,0:T(4,128)S(1)}, f32[4,128]{1,0:T(4,128)}, u32[]{:S(2)}) copy-start(f32[4,128]{1,0:T(4,128)} %param.30) | copy-start | bytes 6148
  403.5 77.2 %copy-start.9 = (s32[1024]{0:T(1024)S(1)}, s32[1024]{0:T(1024)}, u32[]{:S(2)}) copy-start(s32[1024]{0:T(1024)} %get-tuple-element.635) | copy-start | bytes 12292
  403.5 77.2 %copy-start.10 = (s32[1024]{0:T(1024)S(1)}, s32[1024]{0:T(1024)}, u32[]{:S(2)}) copy-start(s32[1024]{0:T(1024)} %get-tuple-element.636) | copy-start | bytes 12292
  403.5 77.2 %copy-start.11 = (f32[1024]{0:T(1024)S(1)}, f32[1024]{0:T(1024)}, u32[]{:S(2)}) copy-start(f32[1024]{0:T(1024)} %get-tuple-element.637) | copy-start | bytes 12292
  403.5 77.2 %copy-start.12 = (f32[1024]{0:T(1024)S(1)}, f32[1024]{0:T(1024)}, u32[]{:S(2)}) copy-start(f32[1024]{0:T(1024)} %get-tuple-element.638) | copy-start | bytes 12292
  403.5 77.2 %copy-start.13 = (f32[1024]{0:T(1024)S(1)}, f32[1024]{0:T(1024)}, u32[]{:S(2)}) copy-start(f32[1024]{0:T(1024)} %get-tuple-element.639) | copy-start | bytes 12292
  403.5 77.2 %copy-start.14 = (f32[1024]{0:T(1024)S(1)}, f32[1024]{0:T(1024)}, u32[]{:S(2)}) copy-start(f32[1024]{0:T(1024)} %get-tuple-element.640) | copy-start | bytes 12292
  403.5 77.2 %copy-start.15 = (f32[1024]{0:T(1024)S(1)}, f32[1024]{0:T(1024)}, u32[]{:S(2)}) copy-start(f32[1024]{0:T(1024)} %get-tuple-element.641) | copy-start | bytes 12292
  403.5 77.2 %copy-start.16 = (f32[1024]{0:T(1024)S(1)}, f32[1024]{0:T(1024)}, u32[]{:S(2)}) copy-start(f32[1024]{0:T(1024)} %get-tuple-element.642) | copy-start | bytes 12292
  403.6 77.2 %copy-start.17 = (f32[1024]{0:T(1024)S(1)}, f32[1024]{0:T(1024)}, u32[]{:S(2)}) copy-start(f32[1024]{0:T(1024)} %get-tuple-element.643) | copy-start | bytes 12292
  403.6 77.2 %copy-start.18 = (f32[1024]{0:T(1024)S(1)}, f32[1024]{0:T(1024)}, u32[]{:S(2)}) copy-start(f32[1024]{0:T(1024)} %get-tuple-element.644) | copy-start | bytes 12292
  403.6 77.2 %copy-start.19 = (f32[1024]{0:T(1024)S(1)}, f32[1024]{0:T(1024)}, u32[]{:S(2)}) copy-start(f32[1024]{0:T(1024)} %get-tuple-element.645) | copy-start | bytes 12292
  403.6 77.2 %copy-start.20 = (f32[1024]{0:T(1024)S(1)}, f32[1024]{0:T(1024)}, u32[]{:S(2)}) copy-start(f32[1024]{0:T(1024)} %get-tuple-element.646) | copy-start | bytes 12292
  403.6 77.2 %copy-start.21 = (f32[1024]{0:T(1024)S(1)}, f32[1024]{0:T(1024)}, u32[]{:S(2)}) copy-start(f32[1024]{0:T(1024)} %get-tuple-element.647) | copy-start | bytes 12292
  403.6 77.2 %copy-start.22 = (f32[1024]{0:T(1024)S(1)}, f32[1024]{0:T(1024)}, u32[]{:S(2)}) copy-start(f32[1024]{0:T(1024)} %get-tuple-element.648) | copy-start | bytes 12292
  403.6 77.2 %copy-start.23 = (f32[1024]{0:T(1024)S(1)}, f32[1024]{0:T(1024)}, u32[]{:S(2)}) copy-start(f32[1024]{0:T(1024)} %get-tuple-element.649) | copy-start | bytes 12292
  403.6 77.2 %copy-start.24 = (f32[1024]{0:T(1024)S(1)}, f32[1024]{0:T(1024)}, u32[]{:S(2)}) copy-start(f32[1024]{0:T(1024)} %get-tuple-element.650) | copy-start | bytes 12292
  403.6 77.2 %copy-start.25 = (f32[1024]{0:T(1024)S(1)}, f32[1024]{0:T(1024)}, u32[]{:S(2)}) copy-start(f32[1024]{0:T(1024)} %get-tuple-element.651) | copy-start | bytes 12292
  403.6 77.2 %copy-start.26 = (f32[1024]{0:T(1024)S(1)}, f32[1024]{0:T(1024)}, u32[]{:S(2)}) copy-start(f32[1024]{0:T(1024)} %get-tuple-element.652) | copy-start | bytes 12292
  403.7 77.2 %copy-start.36 = (s32[256]{0:T(256)S(1)}, s32[256]{0:T(256)}, u32[]{:S(2)}) copy-start(s32[256]{0:T(256)} %iota_add_fusion.1) | copy-start | bytes 3076
  403.7 2.8 collective-permute-start
  405.0 5.7 %collective-permute-start.1 = (bf16[8,1024]{1,0:T(8,128)(2,1)S(1)}, bf16[8,1024]{1,0:T(8,128)(2,1)S(1)}, u32[]{:S(2)}, u32[]{:S(2)}) collective-permute-start(bf16[8,1024]{1,0:T(8,128)(2,1)S(1)} %get-tuple-element.621), channel_id=1, source_target_pairs={{8,0},{16,8},{24,16},{9,1},{17,9},{25,17},{10,2},{18,10},{26,18},{... | collective-permute-start | bytes 49160 | tf_op jit(solution)/shard_map/ppermute | solution.py:36
  (5 other events, 30.5 us)
Sparse Core Ops, SparseCore 0:
  20.0 45.9 all-gather.23
  67.5 44.4 all-gather.21
  113.8 25.3 all-gather.31
  140.9 26.4 all-gather.35
  168.9 46.0 all-gather.25
  216.4 44.4 all-gather.27
  262.5 26.7 all-gather.39
  290.9 27.3 all-gather.41
  319.8 80.1 all-gather.33
  401.4 79.2 all-gather.37
  482.2 44.1 all-gather.29
  529.9 7.1 reduce-scatter.1
where the time goes:
time: 545 us; the launch traced here: 544 us
  waiting for transfers between devices  359 us (66%)
  blocking collectives  93.4 us (17%)
  matrix products  34.2 us (6%)
  other arithmetic  26.8 us (5%)
  between operations  15 us (3%)
  local copies, waits for them, and re-layouts  12.1 us (2%)
    all_gather x1, waiting for transfers between devices, per_device(): lax.all_gather(line_pool_out, 'sp', axis=0, tiled=True)  69.9 us
    all_gather x1, waiting for transfers between devices, per_device(): lax.all_gather(line_pool, 'sp', axis=0, tiled=True)  63.9 us
    all_gather x1, waiting for transfers between devices, per_device(): lax.all_gather(line_value, 'sp', axis=0, tiled=True)  43.7 us
    all_gather x2, waiting for transfers between devices, carried_in(): everything = jax.tree.map(lambda part: lax.all_gather(part, axis), x)  42.1 us
    all_gather x1, waiting for transfers between devices, per_device(): lax.all_gather(line_mem_out, 'sp', axis=0, tiled=True)  40.3 us
    all_gather x1, waiting for transfers between devices, per_device(): lax.all_gather(line_outgate, 'sp', axis=0, tiled=True)  31.8 us
    all_gather x1, waiting for transfers between devices, per_device(): lax.all_gather(pool_out_weight, 'fs', axis=0, tiled=True)  28.2 us
    all_gather x2, blocking collectives, carried_in(): everything = jax.tree.map(lambda part: lax.all_gather(part, axis), x)  24.6 us
  transfers between devices with their start and end apart: 14, of which 12 were waited for; matrix products, arithmetic and copies ran while one was open for 13% of the time, Pallas kernels for 0%

commit v1 on v0

--- a/solution.py
+++ b/solution.py
@@ -7,6 +7,27 @@
 HALO = 8
 norm_eps = 1e-06
 exact_mode = lax.Precision.HIGHEST
+
+
+def ring_gather(shard, axis, dim):
+    count, place, span = (lax.axis_size(axis), lax.axis_index(axis), shard.shape[dim])
+    upward = [(i, (i + 1) % count) for i in range(count)]
+    left = [(i, (i - 1) % count) for i in range(count)]
+    out = jnp.zeros((*shard.shape[:dim], count * span, *shard.shape[dim + 1 :]), shard.dtype)
+    out = lax.dynamic_update_slice_in_dim(out, shard, place * span, axis=dim)
+    from_left = from_right = shard
+    middle = count // 2
+    for turn in range(1, middle + 1):
+        from_left = lax.ppermute(from_left, axis, upward)
+        out = lax.dynamic_update_slice_in_dim(
+            out, from_left, (place - turn) % count * span, axis=dim
+        )
+        if turn < count - middle:
+            from_right = lax.ppermute(from_right, axis, left)
+            out = lax.dynamic_update_slice_in_dim(
+                out, from_right, (place + turn) % count * span, axis=dim
+            )
+    return out
 
 
 def carried_in(x, axis, combine, identity, reverse):
@@ -204,7 +225,7 @@
         lax.all_gather(line_query, "sp", axis=0, tiled=True),
         lax.all_gather(line_key, "sp", axis=0, tiled=True),
         lax.all_gather(line_value, "sp", axis=0, tiled=True),
-        lax.all_gather(line_outgate, "sp", axis=0, tiled=True),
+        ring_gather(line_outgate, "sp", 0),
         lax.all_gather(line_pool, "sp", axis=0, tiled=True),
         lax.all_gather(line_mem_out, "sp", axis=0, tiled=True),
         lax.all_gather(line_pool_out, "sp", axis=0, tiled=True),

time: 545 us -> 523 us (0.960)
  waiting for transfers between devices: 359 us -> 311 us
  blocking collectives: 93.4 us -> 112 us
    all_gather x2, waiting for transfers between devices: 42.1 us -> 3.41 us  [carried_in(): everything = jax.tree.map(lambda part: lax.all_gather(part, axis), x)]
    all_gather x1 -> x0, waiting for transfers between devices: 31.8 us -> none  [per_device(): lax.all_gather(line_outgate, 'sp', axis=0, tiled=True)]
    unnamed x1, blocking collectives: 12.3 us -> 32.5 us
    all_gather x1, waiting for transfers between devices: 8.72 us -> 20.2 us  [per_device(): lax.all_gather(line_key, 'sp', axis=0, tiled=True)]
    ppermute x0 -> x3, waiting for transfers between devices: none -> 11 us  [the longest x2 11 us: ring_gather(): from_left = lax.ppermute(from_left, axis, upward)]
  transfers between devices with their start and end apart: 14 -> 16, of which waited for: 12 -> 11; matrix products, arithmetic and copies ran while one was open for 13% -> 14% of each run, Pallas kernels for 0% -> 0%
where the time goes in v1:
time: 523 us; the launch traced here: 521 us
  waiting for transfers between devices  311 us (59%)
  blocking collectives  112 us (21%)
  matrix products  33 us (6%)
  other arithmetic  27 us (5%)
  local copies, waits for them, and re-layouts  16.1 us (3%)
  between operations  14.8 us (3%)
  starting transfers between devices  6.84 us (1%)
    all_gather x1, waiting for transfers between devices, per_device(): lax.all_gather(line_pool_out, 'sp', axis=0, tiled=True)  70 us
    all_gather x1, waiting for transfers between devices, per_device(): lax.all_gather(line_pool, 'sp', axis=0, tiled=True)  63.9 us
    all_gather x1, waiting for transfers between devices, per_device(): lax.all_gather(line_value, 'sp', axis=0, tiled=True)  43.7 us
    all_gather x1, waiting for transfers between devices, per_device(): lax.all_gather(line_mem_out, 'sp', axis=0, tiled=True)  40.1 us
    unnamed x1, blocking collectives  32.5 us
    all_gather x1, waiting for transfers between devices, per_device(): lax.all_gather(pool_out_weight, 'fs', axis=0, tiled=True)  28.2 us
    all_gather x2, blocking collectives, carried_in(): everything = jax.tree.map(lambda part: lax.all_gather(part, axis), x)  24.4 us
    all_gather x1, waiting for transfers between devices, per_device(): lax.all_gather(line_key, 'sp', axis=0, tiled=True)  20.2 us
  transfers between devices with their start and end apart: 16, of which 11 were waited for; matrix products, arithmetic and copies ran while one was open for 14% of the time, Pallas kernels for 0%

profile of v1, /device:TPU:0, one launch (start us, length us, event | category | flops | bytes accessed | tf_op | source)
XLA Modules:
  0.0 520.8 jit_solution(9403060173089352101)
XLA Ops:
  6.6 13.3 %all_gather.86 = bf16[512,512]{1,0:T(8,128)(2,1)} all-gather(bf16[128,512]{1,0:T(8,128)(2,1)} %param.22), channel_id=1, replica_groups=mesh['sp'=4,'fs'=4,'tp'=2] {'fs'}, dimensions={0}, use_global_device_ids=true | all-gather | bytes 655360 | tf_op jit(solution)/shard_map/all_gather | solution.py:217
  20.0 11.4 %all_gather.84 = bf16[512,512]{1,0:T(8,128)(2,1)} all-gather(bf16[128,512]{1,0:T(8,128)(2,1)} %param.23), channel_id=1, replica_groups=mesh['sp'=4,'fs'=4,'tp'=2] {'fs'}, dimensions={0}, use_global_device_ids=true | all-gather | bytes 655360 | tf_op jit(solution)/shard_map/all_gather | solution.py:218
  32.8 9.8 %all_gather.92 = bf16[512,512]{1,0:T(8,128)(2,1)} all-gather(bf16[128,512]{1,0:T(8,128)(2,1)S(1)} %copy-done.3), channel_id=1, replica_groups=mesh['sp'=4,'fs'=4,'tp'=2] {'fs'}, dimensions={0}, use_global_device_ids=true | all-gather | bytes 655360 | tf_op jit(solution)/shard_map/all_gather | solution.py:216
  43.7 1.2 reduce-window.24
  45.8 20.2 %all-gather.23.cloned.1.call-done = bf16[2048,512]{1,0:T(8,128)(2,1)} async-done(((bf16[512,512]{1,0:T(8,128)(2,1)}), bf16[2048,512]{1,0:T(8,128)(2,1)}) %all-gather.23.cloned.1.call-update) | async-done | bytes 2097168 | tf_op jit(solution)/shard_map/all_gather | solution.py:226
  66.0 2.3 fusion.36
  68.3 43.7 %all-gather.21.cloned.1.call-done = bf16[2048,512]{1,0:T(8,128)(2,1)} async-done(((bf16[512,512]{1,0:T(8,128)(2,1)}), bf16[2048,512]{1,0:T(8,128)(2,1)}) %all-gather.21.cloned.1.call-update) | async-done | bytes 2097168 | tf_op jit(solution)/shard_map/all_gather | solution.py:227
  112.1 2.3 fusion.35
  114.4 1.9 fusion.71
  116.6 1.2 reduce-window.26
  119.6 1.9 fusion.65
  121.6 17.6 %all-gather.29.cloned.1.call-done = bf16[512,1024]{1,0:T(8,128)(2,1)} async-done(((bf16[128,1024]{1,0:T(8,128)(2,1)}), bf16[512,1024]{1,0:T(8,128)(2,1)}) %all-gather.29.cloned.1.call-update) | async-done | bytes 1048592 | tf_op jit(solution)/shard_map/all_gather | solution.py:220
  139.3 28.2 %all-gather.33.cloned.1.call-done = bf16[512,1024]{1,0:T(8,128)(2,1)} async-done(((bf16[128,1024]{1,0:T(8,128)(2,1)}), bf16[512,1024]{1,0:T(8,128)(2,1)}) %all-gather.33.cloned.1.call-update) | async-done | bytes 1048592 | tf_op jit(solution)/shard_map/all_gather | solution.py:222
  167.5 10.1 %all_gather.101 = bf16[512,512]{1,0:T(8,128)(2,1)S(1)} all-gather(bf16[128,512]{1,0:T(8,128)(2,1)S(1)} %copy-done.4), channel_id=1, replica_groups=mesh['sp'=4,'fs'=4,'tp'=2] {'fs'}, dimensions={0}, use_global_device_ids=true | all-gather | bytes 655360 | tf_op jit(solution)/shard_map/all_gather | solution.py:219
  177.6 1.5 collective-permute-start
  179.1 2.3 collective-permute-start.1
  181.4 10.5 %all_gather.102 = bf16[512,512]{1,0:T(8,128)(2,1)} all-gather(bf16[128,512]{1,0:T(8,128)(2,1)S(1)} %copy-done.5), channel_id=1, replica_groups=mesh['sp'=4,'fs'=4,'tp'=2] {'fs'}, dimensions={0}, use_global_device_ids=true | all-gather | bytes 655360 | tf_op jit(solution)/shard_map/all_gather | solution.py:221
  197.9 32.5 %all-reduce.4 = (f32[16]{0:T(128)S(1)}, f32[16]{0:T(128)S(1)}, f32[16]{0:T(128)S(1)}, f32[16]{0:T(128)S(1)}) all-reduce(f32[16]{0:T(128)S(1)} %dynamic-update-slice.2, f32[16]{0:T(128)S(1)} %dynamic-update-slice.3, f32[16]{0:T(128)S(1)} %dynamic-update-slice, f32[16]{0:T(128)S(1)} %dynamic-update-slice.1), channel_id=6, replica_groups=mesh['sp'=4,'fs'=4,'tp'=2] {'sp'}, use_global_device_ids=true, to_apply=%add.2 | all-reduce | flops 64 | bytes 512
  235.3 1.1 constant_dynamic-update-slice_fusion.1
  236.4 11.0 %collective-permute-done.2 = bf16[512,512]{1,0:T(8,128)(2,1)S(1)} collective-permute-done((bf16[512,512]{1,0:T(8,128)(2,1)S(1)}, bf16[512,512]{1,0:T(8,128)(2,1)S(1)}, u32[]{:S(2)}, u32[]{:S(2)}) %collective-permute-start.2) | collective-permute-done | bytes 524320 | tf_op jit(solution)/shard_map/ppermute | solution.py:21
  248.5 1.3 fusion.70
  249.8 12.3 %all-gather.8 = f32[4,4,128]{2,1,0:T(4,128)S(1)} all-gather(f32[1,4,128]{2,1,0:T(4,128)S(1)} %bitcast.306), channel_id=5, replica_groups=mesh['sp'=4,'fs'=4,'tp'=2] {'sp'}, dimensions={0}, use_global_device_ids=true | all-gather | bytes 10240 | tf_op jit(solution)/shard_map/all_gather | solution.py:35
  262.6 12.1 %all-gather.9 = f32[4,4,128]{2,1,0:T(4,128)S(1)} all-gather(f32[1,4,128]{2,1,0:T(4,128)S(1)} %bitcast.302), channel_id=9, replica_groups=mesh['sp'=4,'fs'=4,'tp'=2] {'sp'}, dimensions={0}, use_global_device_ids=true | all-gather | bytes 10240 | tf_op jit(solution)/shard_map/all_gather | solution.py:35
  274.7 2.5 fusion.37
  277.9 3.2 rev.25
  281.1 7.5 %while.12 = (s32[]{:T(128)}, f32[4,128,128]{2,1,0:T(8,128)S(1)}, f32[4,128]{1,0:T(4,128)S(1)}, f32[4]{0:T(128)S(1)}, f32[4]{0:T(128)S(1)}, /*index=5*/s32[]{:T(1...) while((s32[]{:T(128)}, f32[4,128,128]{2,1,0:T(8,128)S(1)}, ...), condition=%wide.region_5.6_spmd.clone, body=%wide.region_4.5_spmd.clone.sunk | while | flops 330284 | bytes 792973 | solution.py:46
  281.8 1.1 fusion.157
  283.7 1.1 fusion.157
  285.6 1.1 fusion.157
  287.4 1.1 fusion.157
  289.8 2.2 fusion.133
  292.0 3.4 all-gather.39.cloned.1.call-done
  295.4 7.5 %while.13 = (s32[]{:T(128)}, f32[4,128,128]{2,1,0:T(8,128)S(1)}, f32[4,128]{1,0:T(4,128)S(1)}, f32[4]{0:T(128)S(1)}, f32[4]{0:T(128)S(1)}, /*index=5*/s32[]{:T(1...) while((s32[]{:T(128)}, f32[4,128,128]{2,1,0:T(8,128)S(1)}, ...), condition=%wide.region_12.13_spmd.clone, body=%wide.region_11.12_spmd.clone.sunk | while | flops 330288 | bytes 793035 | solution.py:46
  296.2 1.1 fusion.159
  301.8 1.1 fusion.159
  304.9 1.2 fusion.25
  306.1 5.1 rev.26
  311.6 1.7 multiply_reduce_fusion
  313.3 63.9 %all-gather.31.cloned.1.call-done = bf16[2048,1024]{1,0:T(8,128)(2,1)} async-done(((bf16[512,1024]{1,0:T(8,128)(2,1)}), bf16[2048,1024]{1,0:T(8,128)(2,1)}) %all-gather.31.cloned.1.call-update) | async-done | bytes 4194320 | tf_op jit(solution)/shard_map/all_gather | solution.py:229
  377.1 3.5 convolution_convert_fusion
  380.8 1.3 collective-permute-start.3
  382.1 1.3 collective-permute-start.4
  383.6 4.2 collective-permute-done.4
  388.0 70.0 %all-gather.35.cloned.1.call-done = bf16[2048,1024]{1,0:T(8,128)(2,1)} async-done(((bf16[512,1024]{1,0:T(8,128)(2,1)}), bf16[2048,1024]{1,0:T(8,128)(2,1)}) %all-gather.35.cloned.1.call-update) | async-done | bytes 4194320 | tf_op jit(solution)/shard_map/all_gather | solution.py:231
  458.1 5.3 %fusion.74 = f32[256,2048]{1,0:T(8,128)S(1)} fusion(bf16[2048,1024]{1,0:T(8,128)(2,1)} %all-gather.35.cloned.1.call-done, f32[272,1024]{1,0:T(8,128)S(1)} %maximum_convert_fusion, s32[1024]{0:T(1024)S(1)} %copy-done.9, s32[1024]{0:T(1024)S(1)} %copy-done.10, s32[256]{0:T(256)S(1)} %copy-done.38, f32[1024]{0:T(1024)S(1)} %copy-done.11, ...), kind=kOutput, calls=%fused_computation.128 | convolution fusion | flops 1084489728 | bytes 23143424 | tf_op jit(solution)/shard_map/dot_general | solution.py:336
  463.5 40.1 %all-gather.27.cloned.1.call-done = bf16[2048,512]{1,0:T(8,128)(2,1)} async-done(((bf16[512,512]{1,0:T(8,128)(2,1)}), bf16[2048,512]{1,0:T(8,128)(2,1)}) %all-gather.27.cloned.1.call-update) | async-done | bytes 2097168 | tf_op jit(solution)/shard_map/all_gather | solution.py:230
  503.6 3.4 fusion.16
  507.0 7.3 %reduce-scatter.2.cloned.1.call-done = bf16[128,2048]{1,0:T(8,128)(2,1)} async-done(((bf16[256,2048]{1,0:T(8,128)(2,1)}), bf16[128,2048]{1,0:T(8,128)(2,1)}) %reduce-scatter.2.cloned.1.call-update) | async-done | bytes 524304 | tf_op jit(solution)/shard_map/reduce_scatter | solution.py:333
  (232 shorter events, 30.1 us)
Async XLA Ops:
  6.5 26.3 %copy-start.3 = (bf16[128,512]{1,0:T(8,128)(2,1)S(1)}, bf16[128,512]{1,0:T(8,128)(2,1)}, u32[]{:S(2)}) copy-start(bf16[128,512]{1,0:T(8,128)(2,1)} %param.21) | copy-start | bytes 393220
  6.5 36.1 %copy-start.6 = (bf16[4,4,2048]{2,1,0:T(4,128)(2,1)S(1)}, bf16[4,4,2048]{2,1,0:T(4,128)(2,1)}, u32[]{:S(2)}) copy-start(bf16[4,4,2048]{2,1,0:T(4,128)(2,1)} %param.25) | copy-start | bytes 196612
  6.5 36.2 %copy-start.28 = (f32[4,4]{1,0:T(4,128)S(1)}, f32[4,4]{1,0:T(4,128)}, u32[]{:S(2)}) copy-start(f32[4,4]{1,0:T(4,128)} %param.26) | copy-start | bytes 196
  6.5 36.3 %copy-start = (bf16[1,256,2048]{2,1,0:T(8,128)(2,1)S(1)}, bf16[1,256,2048]{2,1,0:T(8,128)(2,1)}, u32[]{:S(2)}) copy-start(bf16[1,256,2048]{2,1,0:T(8,128)(2,1)} %param.19) | copy-start | bytes 3145732
  6.5 59.4 %all-gather.23.cloned.1.call-start = ((), (), s32[]{:S(2)}) async-start(), calls=%async_computation.2 | async-start | bytes 2621440 | tf_op jit(solution)/shard_map/all_gather | solution.py:226
  19.9 23.2 %copy-start.35 = (f32[2048]{0:T(1024)S(1)}, f32[2048]{0:T(1024)}, u32[]{:S(2)}) copy-start(f32[2048]{0:T(1024)} %param.20) | copy-start | bytes 24580
  19.9 92.1 %all-gather.21.cloned.1.call-start = ((), (), s32[]{:S(2)}) async-start(), calls=%async_computation.1 | async-start | bytes 2621440 | tf_op jit(solution)/shard_map/all_gather | solution.py:227
  31.4 107.8 %all-gather.29.cloned.1.call-start = ((), (), s32[]{:S(2)}) async-start(), calls=%async_computation.5 | async-start | bytes 1310720 | tf_op jit(solution)/shard_map/all_gather | solution.py:220
  32.1 135.3 %all-gather.33.cloned.1.call-start = ((), (), s32[]{:S(2)}) async-start(), calls=%async_computation.7 | async-start | bytes 1310720 | tf_op jit(solution)/shard_map/all_gather | solution.py:222
  32.7 241.9 %all-gather.25.cloned.1.call-start = ((), (), s32[]{:S(2)}) async-start(), calls=%async_computation.3 | async-start | bytes 2621440 | tf_op jit(solution)/shard_map/all_gather | solution.py:225
  42.6 238.5 %all-gather.37.cloned.1.call-start = ((), (), s32[]{:S(2)}) async-start(), calls=%async_computation.10 | async-start | bytes 1310720 | tf_op jit(solution)/shard_map/all_gather | solution.py:35
  43.1 68.9 %copy-start.30 = (f32[256]{0:T(256)}, f32[256]{0:T(256)S(1)}, u32[]{:S(2)}) copy-start(f32[256]{0:T(256)S(1)} %add_rsqrt_fusion.1) | copy-start | bytes 3076
  68.3 50.5 %copy-start.2 = (bf16[32,4,8,128]{3,2,1,0:T(8,128)(2,1)}, bf16[32,4,8,128]{3,2,1,0:T(8,128)(2,1)S(1)}, u32[]{:S(2)}) copy-start(bf16[32,4,8,128]{3,2,1,0:T(8,128)(2,1)S(1)} %fusion.36) | copy-start | bytes 786436
  116.3 179.1 %all-gather.39.cloned.1.call-start = ((), (), s32[]{:S(2)}) async-start(), calls=%async_computation.11 | async-start | bytes 1310720 | tf_op jit(solution)/shard_map/all_gather | solution.py:35
  119.0 48.6 %copy-start.4 = (bf16[128,512]{1,0:T(8,128)(2,1)S(1)}, bf16[128,512]{1,0:T(8,128)(2,1)}, u32[]{:S(2)}) copy-start(bf16[128,512]{1,0:T(8,128)(2,1)} %param.24) | copy-start | bytes 393220
  119.3 62.2 %copy-start.5 = (bf16[128,512]{1,0:T(8,128)(2,1)S(1)}, bf16[128,512]{1,0:T(8,128)(2,1)}, u32[]{:S(2)}) copy-start(bf16[128,512]{1,0:T(8,128)(2,1)} %param.32) | copy-start | bytes 393220
  121.5 74.3 %copy-start.39 = (u32[32]{0:T(128)S(1)}, u32[32]{0:T(128)}, u32[]{:S(2)}) copy-start(u32[32]{0:T(128)} %constant.242) | copy-start | bytes 388
  121.5 255.6 %all-gather.31.cloned.1.call-start = ((), (), s32[]{:S(2)}) async-start(), calls=%async_computation.6 | async-start | bytes 5242880 | tf_op jit(solution)/shard_map/all_gather | solution.py:229
  139.3 318.7 %all-gather.35.cloned.1.call-start = ((), (), s32[]{:S(2)}) async-start(), calls=%async_computation.8 | async-start | bytes 5242880 | tf_op jit(solution)/shard_map/all_gather | solution.py:231
  167.5 336.1 %all-gather.27.cloned.1.call-start = ((), (), s32[]{:S(2)}) async-start(), calls=%async_computation.4 | async-start | bytes 2621440 | tf_op jit(solution)/shard_map/all_gather | solution.py:230
  177.6 56.4 %collective-permute-start = (bf16[512,512]{1,0:T(8,128)(2,1)S(1)}, bf16[512,512]{1,0:T(8,128)(2,1)S(1)}, u32[]{:S(2)}, u32[]{:S(2)}) collective-permute-start(bf16[512,512]{1,0:T(8,128)(2,1)S(1)} %all_gather.101), channel_id=1, source_target_pairs={{0,8},{8,16},{16,24},{24,0},{1,9},{9,17},{17,25},{25,1},{2,10},{10... | collective-permute-start | bytes 1572872 | tf_op jit(solution)/shard_map/ppermute | solution.py:21
  179.1 56.2 %collective-permute-start.1 = (bf16[512,512]{1,0:T(8,128)(2,1)S(1)}, bf16[512,512]{1,0:T(8,128)(2,1)}, u32[]{:S(2)}, u32[]{:S(2)}) collective-permute-start(bf16[512,512]{1,0:T(8,128)(2,1)S(1)} %all_gather.101), channel_id=1, source_target_pairs={{0,24},{8,0},{16,8},{24,16},{1,25},{9,1},{17,9},{25,17},{2,26},{10... | collective-permute-start | bytes 1572872 | tf_op jit(solution)/shard_map/ppermute | solution.py:26
  192.0 322.4 %reduce-scatter.2.cloned.1.call-start = ((), (), s32[]{:S(2)}) async-start(), calls=%async_computation.9 | async-start | bytes 1572864 | tf_op jit(solution)/shard_map/reduce_scatter | solution.py:333
  234.0 13.4 %collective-permute-start.2 = (bf16[512,512]{1,0:T(8,128)(2,1)S(1)}, bf16[512,512]{1,0:T(8,128)(2,1)S(1)}, u32[]{:S(2)}, u32[]{:S(2)}) collective-permute-start(bf16[512,512]{1,0:T(8,128)(2,1)S(1)} %collective-permute-done), channel_id=1, source_target_pairs={{0,8},{8,16},{16,24},{24,0},{1,9},{9,17},{17,25},{25,1},{2,10},{10... | collective-permute-start | bytes 1572872 | tf_op jit(solution)/shard_map/ppermute | solution.py:21
  311.3 65.8 %copy-start.32 = (f32[256]{0:T(256)S(1)}, f32[256]{0:T(256)}, u32[]{:S(2)}) copy-start(f32[256]{0:T(256)} %copy-done.30) | copy-start | bytes 3076
  311.3 65.8 %copy-start.37 = (f32[2048]{0:T(1024)S(1)}, f32[2048]{0:T(1024)}, u32[]{:S(2)}) copy-start(f32[2048]{0:T(1024)} %param.20) | copy-start | bytes 24580
  313.3 70.2 %copy-start.27 = (f32[4,128]{1,0:T(4,128)S(1)}, f32[4,128]{1,0:T(4,128)}, u32[]{:S(2)}) copy-start(f32[4,128]{1,0:T(4,128)} %param.30) | copy-start | bytes 6148
  380.6 77.3 %copy-start.9 = (s32[1024]{0:T(1024)S(1)}, s32[1024]{0:T(1024)}, u32[]{:S(2)}) copy-start(s32[1024]{0:T(1024)} %get-tuple-element.635) | copy-start | bytes 12292
  380.6 77.3 %copy-start.10 = (s32[1024]{0:T(1024)S(1)}, s32[1024]{0:T(1024)}, u32[]{:S(2)}) copy-start(s32[1024]{0:T(1024)} %get-tuple-element.636) | copy-start | bytes 12292
  380.6 77.3 %copy-start.11 = (f32[1024]{0:T(1024)S(1)}, f32[1024]{0:T(1024)}, u32[]{:S(2)}) copy-start(f32[1024]{0:T(1024)} %get-tuple-element.637) | copy-start | bytes 12292
  380.7 77.3 %copy-start.12 = (f32[1024]{0:T(1024)S(1)}, f32[1024]{0:T(1024)}, u32[]{:S(2)}) copy-start(f32[1024]{0:T(1024)} %get-tuple-element.638) | copy-start | bytes 12292
  380.7 77.3 %copy-start.13 = (f32[1024]{0:T(1024)S(1)}, f32[1024]{0:T(1024)}, u32[]{:S(2)}) copy-start(f32[1024]{0:T(1024)} %get-tuple-element.639) | copy-start | bytes 12292
  380.7 77.3 %copy-start.14 = (f32[1024]{0:T(1024)S(1)}, f32[1024]{0:T(1024)}, u32[]{:S(2)}) copy-start(f32[1024]{0:T(1024)} %get-tuple-element.640) | copy-start | bytes 12292
  380.7 77.3 %copy-start.15 = (f32[1024]{0:T(1024)S(1)}, f32[1024]{0:T(1024)}, u32[]{:S(2)}) copy-start(f32[1024]{0:T(1024)} %get-tuple-element.641) | copy-start | bytes 12292
  380.7 77.3 %copy-start.16 = (f32[1024]{0:T(1024)S(1)}, f32[1024]{0:T(1024)}, u32[]{:S(2)}) copy-start(f32[1024]{0:T(1024)} %get-tuple-element.642) | copy-start | bytes 12292
  380.7 77.3 %copy-start.17 = (f32[1024]{0:T(1024)S(1)}, f32[1024]{0:T(1024)}, u32[]{:S(2)}) copy-start(f32[1024]{0:T(1024)} %get-tuple-element.643) | copy-start | bytes 12292
  380.7 77.3 %copy-start.18 = (f32[1024]{0:T(1024)S(1)}, f32[1024]{0:T(1024)}, u32[]{:S(2)}) copy-start(f32[1024]{0:T(1024)} %get-tuple-element.644) | copy-start | bytes 12292
  380.7 77.3 %copy-start.19 = (f32[1024]{0:T(1024)S(1)}, f32[1024]{0:T(1024)}, u32[]{:S(2)}) copy-start(f32[1024]{0:T(1024)} %get-tuple-element.645) | copy-start | bytes 12292
  380.7 77.3 %copy-start.20 = (f32[1024]{0:T(1024)S(1)}, f32[1024]{0:T(1024)}, u32[]{:S(2)}) copy-start(f32[1024]{0:T(1024)} %get-tuple-element.646) | copy-start | bytes 12292
  380.7 77.3 %copy-start.21 = (f32[1024]{0:T(1024)S(1)}, f32[1024]{0:T(1024)}, u32[]{:S(2)}) copy-start(f32[1024]{0:T(1024)} %get-tuple-element.647) | copy-start | bytes 12292
  380.8 77.3 %copy-start.22 = (f32[1024]{0:T(1024)S(1)}, f32[1024]{0:T(1024)}, u32[]{:S(2)}) copy-start(f32[1024]{0:T(1024)} %get-tuple-element.648) | copy-start | bytes 12292
  380.8 77.3 %copy-start.23 = (f32[1024]{0:T(1024)S(1)}, f32[1024]{0:T(1024)}, u32[]{:S(2)}) copy-start(f32[1024]{0:T(1024)} %get-tuple-element.649) | copy-start | bytes 12292
  380.8 77.3 %copy-start.24 = (f32[1024]{0:T(1024)S(1)}, f32[1024]{0:T(1024)}, u32[]{:S(2)}) copy-start(f32[1024]{0:T(1024)} %get-tuple-element.650) | copy-start | bytes 12292
  380.8 77.3 %copy-start.25 = (f32[1024]{0:T(1024)S(1)}, f32[1024]{0:T(1024)}, u32[]{:S(2)}) copy-start(f32[1024]{0:T(1024)} %get-tuple-element.651) | copy-start | bytes 12292
  380.8 77.3 %copy-start.26 = (f32[1024]{0:T(1024)S(1)}, f32[1024]{0:T(1024)}, u32[]{:S(2)}) copy-start(f32[1024]{0:T(1024)} %get-tuple-element.652) | copy-start | bytes 12292
  380.8 77.3 %copy-start.38 = (s32[256]{0:T(256)S(1)}, s32[256]{0:T(256)}, u32[]{:S(2)}) copy-start(s32[256]{0:T(256)} %iota_add_fusion.1) | copy-start | bytes 3076
  380.8 2.8 collective-permute-start.3
  382.1 5.7 %collective-permute-start.4 = (bf16[8,1024]{1,0:T(8,128)(2,1)S(1)}, bf16[8,1024]{1,0:T(8,128)(2,1)S(1)}, u32[]{:S(2)}, u32[]{:S(2)}) collective-permute-start(bf16[8,1024]{1,0:T(8,128)(2,1)S(1)} %get-tuple-element.621), channel_id=1, source_target_pairs={{8,0},{16,8},{24,16},{9,1},{17,9},{25,17},{10,2},{18,10},{26,18},{... | collective-permute-start | bytes 49160 | tf_op jit(solution)/shard_map/ppermute | solution.py:57
  (9 other events, 82.7 us)
Sparse Core Ops, SparseCore 0:
  20.0 45.9 all-gather.22
  67.6 44.4 all-gather.20
  113.9 25.2 all-gather.28
  140.9 26.4 all-gather.32
  168.9 68.8 all-gather.24
  239.2 27.1 all-gather.36
  268.0 27.3 all-gather.38
  297.0 80.1 all-gather.30
  378.7 79.2 all-gather.34
  459.4 44.1 all-gather.26
  507.1 7.1 reduce-scatter.1
